TPU v7x, 256 devices: a 2x2x32 block of a 4x8x32 slice. The times are simulated.
256 devices in a mesh: grp: 4 (over y, x), ep: 32 (over z), tp: 2 (over core).
Axes of the slice: x: 2, y: 2, z: 32, core: 2. Of those that a mesh axis runs over, the one named last changes fastest.
The devices are a block of a 4x8x32 slice.
Arguments:
- tokens: bfloat16 [16384, 4096], P(('grp', 'ep')), parts along dimension 0, may hold values from -16 to 16, as said below
- norm_gain: float32 [4096], replicated, may hold values from 0.1 to 1.9
- gate_weight: bfloat16 [32, 4096, 768], P('ep', None, 'tp'), may hold values from -0.09375 to 0.09375
- up_weight: bfloat16 [32, 4096, 768], P('ep', None, 'tp'), may hold values from -0.09375 to 0.09375
- down_weight: bfloat16 [32, 768, 4096], P('ep', 'tp'), may hold values from -0.21875 to 0.21875
- chosen: int32 [128, 32, 20], P(('grp', 'ep')), parts along dimension 0, may hold values from 0 to 128, as said below
- affinity: float32 [128, 32, 20], P(('grp', 'ep')), parts along dimension 0, may hold values from 0.2 to 1
Outputs:
- mixed: bfloat16 [16384, 4096], P(('grp', 'ep'), 'tp'), parts along dimension 0
There are 4 independent parts, one for each index of `grp`. A program takes and returns all parts, laid end to end along the dimension named above; an argument that names none is the same for every part. Nothing has to cross between parts.
Inputs may be any that keep to these rules, and one draw needn't show every extreme that they name: `tokens`: draws differ in their scale from row to row. `chosen`: in each (block, expert) row the live entries come first and are distinct; dead entries equal 128. Every expert has exactly 512 live slots in all and at least one live slot in every block; some block gives some expert exactly 20 live slots.
All inputs are finite; a program needn't handle non-finite values.
Results may differ from a plain program's by a relative error of at most 0.0095.
Values may be sent and summed in bfloat16 or wider, within the bound.
A program may use at most 64 MiB of HBM per device.

v0:
```python
import jax
import jax.numpy as jnp
from jax import lax
from jax.sharding import PartitionSpec as P

norm_eps = 1e-06


def cut_along(shard, dim, size):
    before, after = (shard.shape[:dim], shard.shape[dim + 1 :])
    return jnp.moveaxis(shard.reshape(*before, size, -1, *after), dim, 0)


def summed_on_arrival(shard, axis, dim):
    size = lax.axis_size(axis)
    pieces = lax.all_to_all(cut_along(shard, dim, size), axis, 0, 0, tiled=True)
    return jnp.sum(pieces.astype(jnp.float32), axis=0)


def normalize(block, norm_gain):
    values = block.astype(jnp.float32)
    scaled = values * lax.rsqrt(jnp.mean(values * values, axis=-1, keepdims=True) + norm_eps)
    return (scaled * norm_gain).astype(jnp.bfloat16)


def shards(tokens, norm_gain, gate_weight, up_weight, down_weight, chosen, affinity):
    tok_rows = tokens.shape[0]
    model_width = tokens.shape[1]
    slot_count = chosen.shape[2]
    picked_rows = chosen[0]
    source = normalize(tokens, norm_gain)
    half_slots = slot_count // 2
    own_slots = lax.dynamic_slice_in_dim(
        picked_rows, lax.axis_index("tp") * half_slots, half_slots, 1
    )
    outgoing = jnp.take(source, own_slots, axis=0, mode="clip")
    landed = lax.all_to_all(outgoing, "ep", split_axis=0, concat_axis=0, tiled=True)
    arrived = lax.all_gather(landed, "tp", axis=1, tiled=True)
    arrived_rows = arrived.reshape(-1, model_width)
    gate_proj = jnp.dot(arrived_rows, gate_weight[0], preferred_element_type=jnp.float32)
    up_value = jnp.dot(arrived_rows, up_weight[0], preferred_element_type=jnp.float32)
    hidden = (jax.nn.silu(gate_proj) * up_value).astype(jnp.bfloat16)
    columns = down_weight[0]
    summed = summed_on_arrival(
        lax.dot_general(
            columns, hidden, (((0,), (1,)), ((), ())), preferred_element_type=jnp.float32
        ).astype(jnp.bfloat16),
        "tp",
        0,
    )
    expert_out = summed.astype(jnp.bfloat16)
    returned = lax.all_to_all(expert_out, "ep", split_axis=1, concat_axis=1, tiled=True)
    weight = jnp.where(picked_rows < tok_rows, affinity[0], 0.0).astype(jnp.bfloat16).reshape(-1)
    flat_picks = picked_rows.reshape(-1)
    matches = flat_picks[None, :] == jnp.arange(tok_rows, dtype=jnp.int32)[:, None]
    combine = jnp.where(matches, weight[None, :], jnp.zeros((), jnp.bfloat16))
    mixed = lax.dot_general(
        combine, returned, (((1,), (1,)), ((), ())), preferred_element_type=jnp.float32
    )
    return mixed.astype(jnp.bfloat16)


def solution(mesh):
    in_specs = (
        P(("grp", "ep"), None),
        P(),
        P("ep", None, "tp"),
        P("ep", None, "tp"),
        P("ep", "tp", None),
        P(("grp", "ep"), None, None),
        P(("grp", "ep"), None, None),
    )
    out_specs = P(("grp", "ep"), "tp")
    return jax.shard_map(shards, mesh=mesh, in_specs=in_specs, out_specs=out_specs, check_vma=False)
```

profile of v0, /device:TPU:357, one launch (start us, length us, event | category | flops | bytes accessed | tf_op | source)
XLA Modules:
  0.0 832.0 jit_solution(3953942204151701795)
XLA Ops:
  6.6 0.8 constant_dynamic-slice_fusion
  7.5 0.1 reshape.35
  7.6 1.5 fusion.5
  9.1 2.5 fusion.7
  11.7 9.4 %gather_fusion = bf16[320,4096]{1,0:T(8,128)(2,1)} fusion(bf16[128,4096]{1,0:T(8,128)(2,1)} %fusion.7, s32[1024]{0:T(1024)S(1)} %pad_clamp_fusion), kind=kCustom, calls=%fused_computation | custom fusion | bytes 5244160 | tf_op jit(solution)/shard_map/jit(_take)/gather | solution.py:36
  21.1 4.6 reshape.34
  25.7 396.9 %all_to_all.22 = bf16[32,10,4096]{2,1,0:T(8,128)(2,1)S(1)} all-to-all(bf16[32,10,4096]{2,1,0:T(8,128)(2,1)} %reshape.34), channel_id=1, replica_groups=mesh['grp'=4,'ep'=32,'tp'=2] {'ep'}, dimensions={0} | all-to-all | bytes 5242880 | tf_op jit(solution)/shard_map/all_to_all | solution.py:37
  422.6 2.9 copy.14
  425.6 26.6 %all-gather.2.cloned.1.call-done = bf16[32,20,4096]{2,0,1:T(8,128)(2,1)} async-done(((bf16[32,10,4096]{2,0,1:T(8,128)(2,1)}), bf16[32,20,4096]{2,0,1:T(8,128)(2,1)}) %all-gather.2.cloned.1.call-update) | async-done | bytes 5242896 | tf_op jit(solution)/shard_map/all_gather | solution.py:38
  452.2 8.1 copy.15
  460.3 7.8 reshape.31
  468.1 7.3 fusion.3
  475.4 11.6 %convolution_convert_fusion = bf16[640,4096]{1,0:T(8,128)(2,1)} fusion(bf16[1,384,4096]{2,1,0:T(8,128)(2,1)S(1)} %copy-done, bf16[640,4096]{1,0:T(8,128)(2,1)} %reshape.31, bf16[1,4096,384]{2,1,0:T(8,128)(2,1)} %param.10, f32[640,384]{1,0:T(8,128)} %fusion.3), kind=kOutput, calls=%fused_computation.1 | convolution fusion | flops 4030627840 | bytes 17760256 | tf_op jit(solution)/shard_map/dot_general | solution.py:45
  487.1 2.9 copy.19
  490.0 9.1 %all_to_all.23 = bf16[2,2048,640]{1,2,0:T(8,128)(2,1)} all-to-all(bf16[2,2048,640]{1,2,0:T(8,128)(2,1)S(1)} %bitcast.27), channel_id=1, replica_groups=mesh['grp'=4,'ep'=32,'tp'=2] {'tp'}, dimensions={0} | all-to-all | bytes 10485760 | tf_op jit(solution)/shard_map/all_to_all | solution.py:16
  499.0 6.0 reduce_sum.22
  505.1 5.1 all_to_all.16
  510.2 22.0 %all-to-all-start.2 = ((bf16[2048,32,20]{0,2,1:T(8,128)(2,1)}), bf16[2048,32,20]{0,2,1:T(8,128)(2,1)}, u32[]{:S(2)}, u32[]{:S(2)}) async-start(bf16[2048,32,20]{0,2,1:T(8,128)(2,1)} %all_to_all.16), calls=%async_computation.2 | async-start | bytes 6291456 | tf_op jit(solution)/shard_map/all_to_all | solution.py:52
  532.3 0.1 eq.15
  532.4 0.1 copy.12
  532.5 0.1 squeeze.13
  532.7 284.1 %all-to-all-done.2 = bf16[2048,32,20]{0,2,1:T(8,128)(2,1)} async-done(((bf16[2048,32,20]{0,2,1:T(8,128)(2,1)}), bf16[2048,32,20]{0,2,1:T(8,128)(2,1)}, u32[]{:S(2)}, u32[]{:S(2)}) %all-to-all-start.2) | async-done | bytes 2621472 | tf_op jit(solution)/shard_map/all_to_all | solution.py:52
  816.8 5.2 all_to_all.18
  822.0 3.1 convolution_convert_fusion.1
  (13 shorter events, 0.3 us)
Async XLA Ops:
  6.5 468.9 %copy-start = (bf16[1,384,4096]{2,1,0:T(8,128)(2,1)S(1)}, bf16[1,384,4096]{2,1,0:T(8,128)(2,1)}, u32[]{:S(2)}) copy-start(bf16[1,384,4096]{2,1,0:T(8,128)(2,1)} %param.11) | copy-start | bytes 9437188
  6.6 445.7 %all-gather.2.cloned.1.call-start = ((), (), s32[]{:S(2)}) async-start(), calls=%async_computation.3 | async-start | bytes 7864320 | tf_op jit(solution)/shard_map/all_gather | solution.py:38
  510.2 22.0 %copy-start.1 = (s32[1,32,20]{1,0,2:T(1,128)S(1)}, s32[1,32,20]{1,0,2:T(1,128)}, u32[]{:S(2)}) copy-start(s32[1,32,20]{1,0,2:T(1,128)} %param.12) | copy-start | bytes 7684
  510.2 22.2 %copy-start.2 = (f32[1,32,20]{1,0,2:T(1,128)S(1)}, f32[1,32,20]{1,0,2:T(1,128)}, u32[]{:S(2)}) copy-start(f32[1,32,20]{1,0,2:T(1,128)} %param.13) | copy-start | bytes 7684
  510.2 306.6 %all-to-all-start.2 = ((bf16[2048,32,20]{0,2,1:T(8,128)(2,1)}), bf16[2048,32,20]{0,2,1:T(8,128)(2,1)}, u32[]{:S(2)}, u32[]{:S(2)}) async-start(bf16[2048,32,20]{0,2,1:T(8,128)(2,1)} %all_to_all.16), calls=%async_computation.2 | async-start | bytes 6291456 | tf_op jit(solution)/shard_map/all_to_all | solution.py:52
Sparse Core Ops, SparseCore 0:
  425.7 26.4 all-gather.1
where the time goes:
time: 833 us; the launch traced here: 832 us
  blocking collectives  406 us (49%)
  waiting for transfers between devices  311 us (37%)
  local copies, waits for them, and re-layouts  47.6 us (6%)
  matrix products  22.1 us (3%)
  starting transfers between devices  22 us (3%)
  between operations  13.5 us (2%)
  other arithmetic  10.1 us (1%)
    all_to_all x1, blocking collectives, shards(): lax.all_to_all(outgoing, 'ep', split_axis=0, concat_axis=0, tiled=True)  397 us
    all_to_all x1, waiting for transfers between devices, shards(): lax.all_to_all(expert_out, 'ep', split_axis=1, concat_axis=1, tiled=True)  284 us
    all_gather x1, waiting for transfers between devices, shards(): arrived = lax.all_gather(landed, 'tp', axis=1, tiled=True)  26.6 us
    all_to_all x1, starting transfers between devices, shards(): lax.all_to_all(expert_out, 'ep', split_axis=1, concat_axis=1, tiled=True)  22 us
  transfers between devices with their start and end apart: 2, of which 2 were waited for; matrix products, arithmetic and copies ran while one was open for 0% of the time, Pallas kernels for 0%

commit v1 on v0

--- a/solution.py
+++ b/solution.py
@@ -35,7 +35,10 @@
     )
     outgoing = jnp.take(source, own_slots, axis=0, mode="clip")
     landed = lax.all_to_all(outgoing, "ep", split_axis=0, concat_axis=0, tiled=True)
-    arrived = lax.all_gather(landed, "tp", axis=1, tiled=True)
+    devices = lax.axis_size("tp")
+    parts = jnp.stack([landed for _ in range(devices)])
+    parts = lax.all_to_all(parts, "tp", split_axis=0, concat_axis=0)
+    arrived = jnp.concatenate(parts, axis=1)
     arrived_rows = arrived.reshape(-1, model_width)
     gate_proj = jnp.dot(arrived_rows, gate_weight[0], preferred_element_type=jnp.float32)
     up_value = jnp.dot(arrived_rows, up_weight[0], preferred_element_type=jnp.float32)

time: 833 us -> 804 us (0.965)
  waiting for transfers between devices: 311 us -> 284 us
  blocking collectives: 406 us -> 420 us
  starting transfers between devices: 22 us -> 8.08 us
  between operations: 13.5 us -> 0.07 us
    all_gather x1 -> x0, waiting for transfers between devices: 26.6 us -> none  [shards(): arrived = lax.all_gather(landed, 'tp', axis=1, tiled=True)]
    another operation x0 -> x2, local copies, waits for them, and re-layouts: none -> 14.9 us  [the longest x1 8.6 us: shards(): arrived_rows = arrived.reshape(-1, model_width)]
    all_to_all x0 -> x1, blocking collectives: none -> 14 us  [shards(): parts = lax.all_to_all(parts, 'tp', split_axis=0, concat_axis=0)]
    all_to_all x1, starting transfers between devices: 22 us -> 8.08 us  [shards(): lax.all_to_all(expert_out, 'ep', split_axis=1, concat_axis=1, tiled=True)]
  transfers between devices with their start and end apart: 2 -> 1, of which waited for: 2 -> 1; matrix products, arithmetic and copies ran while one was open for 0% -> 0% of each run, Pallas kernels for 0% -> 0%
where the time goes in v1:
time: 804 us; the launch traced here: 803 us
  blocking collectives  420 us (52%)
  waiting for transfers between devices  284 us (35%)
  local copies, waits for them, and re-layouts  50 us (6%)
  matrix products  22 us (3%)
  other arithmetic  17.9 us (2%)
  starting transfers between devices  8.08 us (1%)
    all_to_all x1, blocking collectives, shards(): lax.all_to_all(outgoing, 'ep', split_axis=0, concat_axis=0, tiled=True)  397 us
    all_to_all x1, waiting for transfers between devices, shards(): lax.all_to_all(expert_out, 'ep', split_axis=1, concat_axis=1, tiled=True)  284 us
  transfers between devices with their start and end apart: 1, of which 1 were waited for; matrix products, arithmetic and copies ran while one was open for 0% of the time, Pallas kernels for 0%

profile of v1, /device:TPU:357, one launch (start us, length us, event | category | flops | bytes accessed | tf_op | source)
XLA Modules:
  0.0 802.5 jit_solution(9883864023244133956)
XLA Ops:
  0.0 0.8 constant_dynamic-slice_fusion
  0.9 0.1 reshape.35
  1.1 1.5 fusion.5
  2.6 2.5 fusion.7
  5.1 9.4 %gather_fusion = bf16[320,4096]{1,0:T(8,128)(2,1)} fusion(bf16[128,4096]{1,0:T(8,128)(2,1)} %fusion.7, s32[1024]{0:T(1024)S(1)} %pad_clamp_fusion), kind=kCustom, calls=%fused_computation | custom fusion | bytes 5244160 | tf_op jit(solution)/shard_map/jit(_take)/gather | solution.py:36
  14.6 4.6 reshape.34
  19.2 397.4 %all_to_all.27 = bf16[32,10,4096]{2,1,0:T(8,128)(2,1)} all-to-all(bf16[32,10,4096]{2,1,0:T(8,128)(2,1)} %reshape.34), channel_id=1, replica_groups=mesh['grp'=4,'ep'=32,'tp'=2] {'ep'}, dimensions={0} | all-to-all | bytes 5242880 | tf_op jit(solution)/shard_map/all_to_all | solution.py:37
  416.6 7.8 pad_maximum_fusion
  424.4 6.2 copy.15
  430.6 14.0 %all_to_all.28 = bf16[2,32,10,4096]{3,1,2,0:T(8,128)(2,1)S(1)} all-to-all(bf16[2,32,10,4096]{3,1,2,0:T(8,128)(2,1)S(1)} %copy.15), channel_id=1, replica_groups=mesh['grp'=4,'ep'=32,'tp'=2] {'tp'}, dimensions={0} | all-to-all | bytes 10485760 | tf_op jit(solution)/shard_map/all_to_all | solution.py:40
  444.6 6.4 copy.16
  451.0 8.6 %reshape_reshape.3 = bf16[640,4096]{1,0:T(8,128)(2,1)} reshape(bf16[32,2,10,4096]{3,2,1,0:T(8,128)(2,1)} %copy.16) | data formatting | bytes 10485760 | tf_op jit(solution)/shard_map/reshape;reshape | solution.py:42
  459.6 7.3 fusion.3
  466.9 11.5 %convolution_convert_fusion = bf16[640,4096]{1,0:T(8,128)(2,1)} fusion(bf16[1,384,4096]{2,1,0:T(8,128)(2,1)S(1)} %copy-done, bf16[640,4096]{1,0:T(8,128)(2,1)} %reshape_reshape.3, bf16[1,4096,384]{2,1,0:T(8,128)(2,1)} %param.10, f32[640,384]{1,0:T(8,128)} %fusion.3), kind=kOutput, calls=%fused_computation.2 | convolution fusion | flops 4030627840 | bytes 17760256 | tf_op jit(solution)/shard_map/dot_general | solution.py:48
  478.5 2.9 copy.20
  481.4 9.0 %all_to_all.29 = bf16[2,2048,640]{1,2,0:T(8,128)(2,1)} all-to-all(bf16[2,2048,640]{1,2,0:T(8,128)(2,1)S(1)} %bitcast.30), channel_id=1, replica_groups=mesh['grp'=4,'ep'=32,'tp'=2] {'tp'}, dimensions={0} | all-to-all | bytes 10485760 | tf_op jit(solution)/shard_map/all_to_all | solution.py:16
  490.4 6.0 reduce_sum.22
  496.4 5.2 all_to_all.20
  501.6 8.1 %all-to-all-start.3 = ((bf16[2048,32,20]{0,2,1:T(8,128)(2,1)}), bf16[2048,32,20]{0,2,1:T(8,128)(2,1)}, u32[]{:S(2)}, u32[]{:S(2)}) async-start(bf16[2048,32,20]{0,2,1:T(8,128)(2,1)} %all_to_all.20), calls=%async_computation.3 | async-start | bytes 6291456 | tf_op jit(solution)/shard_map/all_to_all | solution.py:55
  509.8 0.1 eq.15
  510.0 0.1 squeeze.13
  510.1 284.1 %all-to-all-done.3 = bf16[2048,32,20]{0,2,1:T(8,128)(2,1)} async-done(((bf16[2048,32,20]{0,2,1:T(8,128)(2,1)}), bf16[2048,32,20]{0,2,1:T(8,128)(2,1)}, u32[]{:S(2)}, u32[]{:S(2)}) %all-to-all-start.3) | async-done | bytes 2621472 | tf_op jit(solution)/shard_map/all_to_all | solution.py:55
  794.2 5.2 all_to_all.22
  799.4 3.1 convolution_convert_fusion.1
  (12 shorter events, 0.3 us)
Async XLA Ops:
  0.0 466.9 %copy-start = (bf16[1,384,4096]{2,1,0:T(8,128)(2,1)S(1)}, bf16[1,384,4096]{2,1,0:T(8,128)(2,1)}, u32[]{:S(2)}) copy-start(bf16[1,384,4096]{2,1,0:T(8,128)(2,1)} %param.11) | copy-start | bytes 9437188
  501.6 8.1 %copy-start.1 = (s32[1,32,20]{1,0,2:T(1,128)S(1)}, s32[1,32,20]{1,0,2:T(1,128)}, u32[]{:S(2)}) copy-start(s32[1,32,20]{1,0,2:T(1,128)} %param.12) | copy-start | bytes 7684
  501.6 8.3 %copy-start.2 = (f32[1,32,20]{1,0,2:T(1,128)S(1)}, f32[1,32,20]{1,0,2:T(1,128)}, u32[]{:S(2)}) copy-start(f32[1,32,20]{1,0,2:T(1,128)} %param.13) | copy-start | bytes 7684
  501.6 292.7 %all-to-all-start.3 = ((bf16[2048,32,20]{0,2,1:T(8,128)(2,1)}), bf16[2048,32,20]{0,2,1:T(8,128)(2,1)}, u32[]{:S(2)}, u32[]{:S(2)}) async-start(bf16[2048,32,20]{0,2,1:T(8,128)(2,1)} %all_to_all.20), calls=%async_computation.3 | async-start | bytes 6291456 | tf_op jit(solution)/shard_map/all_to_all | solution.py:55
